TPU v7x, 32 devices: a whole 2x2x4 slice. The times are simulated.
32 devices in a mesh: rep: 2 (over x), fs: 8 (over z, y), tp: 2 (over core).
Axes of the slice: x: 2, y: 2, z: 4, core: 2. Of those that a mesh axis runs over, the one named last changes fastest.
Arguments:
- incoming_features: bfloat16 [3072, 2048], P(('rep', 'fs'), 'tp'), may hold values from -6 to 6
- attend_prenormal_scale: bfloat16 [2048], replicated, may hold values from 0.099609375 to 1.8984375
- probe_matrix: bfloat16 [2048, 512], P('fs', 'tp'), may hold values from -0.125 to 0.125
- lookup_matrix: bfloat16 [2048, 512], P('fs', 'tp'), may hold values from -0.125 to 0.125
- content_matrix: bfloat16 [2048, 1024], P('fs', 'tp'), may hold values from -0.125 to 0.125
- forgetting_matrix: bfloat16 [2048, 512], P('fs', 'tp'), may hold values from -0.125 to 0.125
- result_switch_matrix: bfloat16 [2048, 1024], P('fs', 'tp'), may hold values from -0.125 to 0.125
- forgetting_shift: float32 [512], P('tp'), may hold values from -0.5 to 5.5
- spike_forget_logarithm: float32 [3072, 512], P(('rep', 'fs'), 'tp'), may hold values from -0.7 to 0
- attend_unit_scale: bfloat16 [1024], P('tp'), may hold values from 0.099609375 to 1.8984375
- attend_result_matrix: bfloat16 [1024, 2048], P('tp', 'fs'), may hold values from -0.1875 to 0.1875
- perceptron_scale: bfloat16 [2048], replicated, may hold values from 0.099609375 to 1.8984375
- content_expand_matrix: bfloat16 [2048, 4096], P('fs', 'tp'), may hold values from -0.125 to 0.125
- switch_expand_matrix: bfloat16 [2048, 4096], P('fs', 'tp'), may hold values from -0.125 to 0.125
- content_kernel: bfloat16 [3, 4096], P(None, 'tp'), may hold values from -3.5 to 3.5
- switch_kernel: bfloat16 [3, 4096], P(None, 'tp'), may hold values from -3.5 to 3.5
- contract_matrix: bfloat16 [4096, 2048], P('tp', 'fs'), may hold values from -0.09375 to 0.09375
Outputs:
- out_rows: bfloat16 [3072, 2048], P(('rep', 'fs'), 'tp')
All inputs are finite; a program needn't handle non-finite values.
Results may differ from a plain program's by a relative error of at most 0.02.
Values may be sent and summed in bfloat16 or wider, within the bound.
A program may use at most 64 MiB of HBM per device.

v0:
```python
import jax
import jax.numpy as jnp
from jax import lax
from jax.sharding import PartitionSpec as P

HEAD_K = 32
HEAD_V = 64
BLOCK = 64
norm_eps = 1e-06
switch_multiplier = 16.0


def row_norm(content_tokens, gain):
    content_tokens = content_tokens.astype(jnp.float32)
    scaled = content_tokens * lax.rsqrt(
        jnp.mean(content_tokens * content_tokens, axis=-1, keepdims=True) + norm_eps
    )
    return (scaled * gain.astype(jnp.float32)).astype(jnp.bfloat16)


def gated_scan(probe_tokens, lookup_tokens, content_tokens, forgetting_scores):
    length, heads, key_size = probe_tokens.shape
    value_size = content_tokens.shape[-1]
    blocks = length // BLOCK

    def split_blocks(array):
        return array.reshape(blocks, BLOCK, heads, array.shape[-1])

    causal = jnp.arange(BLOCK)[:, None] >= jnp.arange(BLOCK)[None, :]
    highest = lax.Precision.HIGHEST

    def step(state, incoming_tokens):
        query_block, key_block, value_block, decay_block = incoming_tokens
        cumulative = jnp.cumsum(decay_block, axis=0)
        differ = cumulative[:, None] - cumulative[None, :]
        weight = jnp.exp(jnp.where(causal[:, :, None, None], differ, -jnp.inf))
        scores = jnp.einsum("thd,shd,tshd->tsh", query_block, key_block, weight, precision=highest)
        inner = jnp.einsum("tsh,shv->thv", scores, value_block, precision=highest)
        carried = jnp.einsum(
            "thd,hdv->thv", query_block * jnp.exp(cumulative), state, precision=highest
        )
        final = cumulative[-1]
        state = jnp.exp(final)[:, :, None] * state + jnp.einsum(
            "shd,shv->hdv",
            key_block * jnp.exp(final[None] - cumulative),
            value_block,
            precision=highest,
        )
        return (state, inner + carried)

    start_state = jnp.zeros((heads, key_size, value_size), jnp.float32)
    _, result_tokens = lax.scan(
        step,
        start_state,
        (
            split_blocks(probe_tokens),
            split_blocks(lookup_tokens),
            split_blocks(content_tokens),
            split_blocks(forgetting_scores),
        ),
    )
    return result_tokens.reshape(length, heads, value_size)


def attend_unit_results(
    probe_tokens,
    lookup_tokens,
    content_tokens,
    result_switch,
    forgetting_raw,
    spike_forgetting,
    attend_unit_scale,
):
    length = probe_tokens.shape[0]
    heads = probe_tokens.shape[1] // HEAD_K
    forgetting_scores = jax.nn.log_sigmoid(forgetting_raw) / switch_multiplier + spike_forgetting

    def split_heads(array, width):
        return array.astype(jnp.float32).reshape(length, heads, width)

    result_tokens = gated_scan(
        split_heads(probe_tokens, HEAD_K) * HEAD_K ** (-0.5),
        split_heads(lookup_tokens, HEAD_K),
        split_heads(content_tokens, HEAD_V),
        split_heads(forgetting_scores, HEAD_K),
    )
    result_tokens = result_tokens * lax.rsqrt(
        jnp.mean(result_tokens * result_tokens, axis=-1, keepdims=True) + norm_eps
    )
    result_tokens = result_tokens * attend_unit_scale.astype(jnp.float32).reshape(heads, HEAD_V)
    switched_result = result_tokens.reshape(length, heads * HEAD_V) * jax.nn.silu(
        result_switch.astype(jnp.float32)
    )
    return switched_result.astype(jnp.bfloat16)


def causal_conv(content_tokens, taps):
    content_tokens = content_tokens.astype(jnp.float32)
    taps = taps.astype(jnp.float32)
    width = taps.shape[0]
    padded = jnp.pad(content_tokens, ((width - 1, 0), (0, 0)))
    total = jnp.zeros_like(content_tokens)
    for offset in range(width):
        total = total + padded[offset : offset + content_tokens.shape[0]] * taps[offset]
    return total


def shards(
    incoming_features,
    attend_prenormal_scale,
    probe_matrix,
    lookup_matrix,
    content_matrix,
    forgetting_matrix,
    result_switch_matrix,
    forgetting_shift,
    spike_forget_logarithm,
    attend_unit_scale,
    attend_result_matrix,
    perceptron_scale,
    content_expand_matrix,
    switch_expand_matrix,
    content_kernel,
    switch_kernel,
    contract_matrix,
):
    whole_in = lax.all_gather(incoming_features, "tp", axis=1, tiled=True)
    normed = row_norm(whole_in, attend_prenormal_scale)
    pieces = (
        lax.all_gather(probe_matrix, "fs", axis=0, tiled=True),
        lax.all_gather(lookup_matrix, "fs", axis=0, tiled=True),
        lax.all_gather(content_matrix, "fs", axis=0, tiled=True),
        lax.all_gather(forgetting_matrix, "fs", axis=0, tiled=True),
        lax.all_gather(result_switch_matrix, "fs", axis=0, tiled=True),
    )
    columns = normed
    query_sum, key_sum, value_sum, decay_sum, gate_sum = tuple(
        (jnp.dot(columns, piece, preferred_element_type=jnp.float32) for piece in pieces)
    )
    switched_result = attend_unit_results(
        query_sum.astype(jnp.bfloat16),
        key_sum.astype(jnp.bfloat16),
        value_sum.astype(jnp.bfloat16),
        gate_sum.astype(jnp.bfloat16),
        decay_sum + forgetting_shift,
        spike_forget_logarithm,
        attend_unit_scale,
    )
    mixer_partial = jnp.dot(
        switched_result,
        lax.all_gather(attend_result_matrix, "fs", axis=1, tiled=True),
        preferred_element_type=jnp.float32,
    )
    mix = lax.psum_scatter(
        mixer_partial.astype(jnp.bfloat16), "tp", scatter_dimension=1, tiled=True
    )
    middle = (
        incoming_features.astype(jnp.float32) + lax.optimization_barrier(mix).astype(jnp.float32)
    ).astype(jnp.bfloat16)
    whole_mid = lax.all_gather(middle, "tp", axis=1, tiled=True)
    normed_mid = row_norm(whole_mid, perceptron_scale)
    pieces = (
        lax.all_gather(content_expand_matrix, "fs", axis=0, tiled=True),
        lax.all_gather(switch_expand_matrix, "fs", axis=0, tiled=True),
    )
    columns = normed_mid
    value_total = jnp.dot(columns, pieces[0], preferred_element_type=jnp.float32)
    gate_total = jnp.dot(columns, pieces[1], preferred_element_type=jnp.float32)
    conv_value = causal_conv(value_total.astype(jnp.bfloat16), content_kernel)
    conv_gated = causal_conv(gate_total.astype(jnp.bfloat16), switch_kernel)
    hidden = (conv_value * jax.nn.gelu(conv_gated, approximate=True)).astype(jnp.bfloat16)
    down_partial = jnp.dot(
        hidden,
        lax.all_gather(contract_matrix, "fs", axis=1, tiled=True),
        preferred_element_type=jnp.float32,
    )
    ffn = lax.psum_scatter(down_partial.astype(jnp.bfloat16), "tp", scatter_dimension=1, tiled=True)
    return (middle.astype(jnp.float32) + lax.optimization_barrier(ffn).astype(jnp.float32)).astype(
        jnp.bfloat16
    )


def solution(mesh):
    placed = (
        P(("rep", "fs"), "tp"),
        P(),
        P("fs", "tp"),
        P("fs", "tp"),
        P("fs", "tp"),
        P("fs", "tp"),
        P("fs", "tp"),
        P("tp"),
        P(("rep", "fs"), "tp"),
        P("tp"),
        P("tp", "fs"),
        P(),
        P("fs", "tp"),
        P("fs", "tp"),
        P(None, "tp"),
        P(None, "tp"),
        P("tp", "fs"),
    )
    return jax.shard_map(
        shards, mesh=mesh, in_specs=placed, out_specs=P(("rep", "fs"), "tp"), check_vma=False
    )
```

profile of v0, /device:TPU:0, one launch (start us, length us, event | category | flops | bytes accessed | tf_op | source)
XLA Modules:
  0.0 697.6 jit_solution(7244822778492802372)
XLA Ops:
  6.6 0.7 all-gather.10.cloned.1.call-update
  7.3 0.7 all-gather.12.cloned.1.call-update
  8.1 0.7 all-gather.16.cloned.1.call-update
  8.8 0.5 all-gather.14.cloned.1.call-update
  9.4 0.5 all-gather.18.cloned.1.call-update
  10.0 0.5 all-gather.20.cloned.1.call-update
  10.6 2.7 all_gather.33
  13.3 0.2 fusion.29
  13.5 39.0 %all-gather.10.cloned.1.call-done = bf16[2048,256]{1,0:T(8,128)(2,1)} async-done(((bf16[256,256]{1,0:T(8,128)(2,1)}), bf16[2048,256]{1,0:T(8,128)(2,1)}) %all-gather.10.cloned.1.call-update) | async-done | bytes 1048592 | tf_op jit(solution)/shard_map/all_gather | solution.py:133
  52.5 1.7 fusion.65
  54.3 1.1 reshape.64
  55.4 38.2 %all-gather.12.cloned.1.call-done = bf16[2048,256]{1,0:T(8,128)(2,1)} async-done(((bf16[256,256]{1,0:T(8,128)(2,1)}), bf16[2048,256]{1,0:T(8,128)(2,1)}) %all-gather.12.cloned.1.call-update) | async-done | bytes 1048592 | tf_op jit(solution)/shard_map/all_gather | solution.py:131
  93.7 1.7 fusion.47
  95.3 0.2 reshape.65
  95.5 39.3 %all-gather.16.cloned.1.call-done = bf16[2048,256]{1,0:T(8,128)(2,1)} async-done(((bf16[256,256]{1,0:T(8,128)(2,1)}), bf16[2048,256]{1,0:T(8,128)(2,1)}) %all-gather.16.cloned.1.call-update) | async-done | bytes 1048592 | tf_op jit(solution)/shard_map/all_gather | solution.py:130
  134.8 1.7 fusion.46
  136.5 0.2 reshape.66
  136.7 47.9 %all-gather.14.cloned.1.call-done = bf16[2048,512]{1,0:T(8,128)(2,1)} async-done(((bf16[256,512]{1,0:T(8,128)(2,1)}), bf16[2048,512]{1,0:T(8,128)(2,1)}) %all-gather.14.cloned.1.call-update) | async-done | bytes 2097168 | tf_op jit(solution)/shard_map/all_gather | solution.py:132
  184.6 2.2 fusion.43
  186.8 1.1 reshape.60
  187.9 73.7 %while.13 = (s32[]{:T(128)}, f32[8,32,64]{2,1,0:T(8,128)S(1)}, f32[3,64,8,64]{1,3,2,0:T(8,128)}, f32[3,64,8,32]{3,2,1,0:T(8,128)}, f32[3,64,8,32]{3,2,1,0:T(8,12...) while((s32[]{:T(128)}, f32[8,32,64]{2,1,0:T(8,128)S(1)}, ...), condition=%wide.region_3.4_spmd.clone, body=%wide.region_1.3_spmd.clone.sunk | while | flops 56725504 | bytes 20003956 | solution.py:52
  187.9 1.0 fusion.106
  189.1 4.7 select_exponential_fusion.2
  193.8 9.5 %copy.122 = f32[64,64,8,32]{0,1,3,2:T(8,128)} copy(f32[64,64,8,32]{1,3,2,0:T(8,128)} %select_exponential_fusion.2) | data formatting | bytes 8388608 | tf_op jit(solution)/shard_map/while
  203.6 5.3 fusion.108
  208.8 1.0 constant_dynamic-slice_fusion.2
  209.8 0.6 convolution_bitcast_fusion.3
  210.5 1.3 fusion.109
  211.9 0.6 convolution_add_fusion.3
  212.5 1.0 fusion.106
  213.7 4.6 select_exponential_fusion.2
  218.3 9.5 %copy.122 = f32[64,64,8,32]{0,1,3,2:T(8,128)} copy(f32[64,64,8,32]{1,3,2,0:T(8,128)} %select_exponential_fusion.2) | data formatting | bytes 8388608 | tf_op jit(solution)/shard_map/while
  228.1 5.2 fusion.108
  233.4 1.0 constant_dynamic-slice_fusion.2
  234.4 0.6 convolution_bitcast_fusion.3
  235.1 1.3 fusion.109
  236.4 0.6 convolution_add_fusion.3
  237.0 1.0 fusion.106
  238.2 4.7 select_exponential_fusion.2
  242.9 9.6 %copy.122 = f32[64,64,8,32]{0,1,3,2:T(8,128)} copy(f32[64,64,8,32]{1,3,2,0:T(8,128)} %select_exponential_fusion.2) | data formatting | bytes 8388608 | tf_op jit(solution)/shard_map/while
  252.8 5.3 fusion.108
  258.0 1.0 constant_dynamic-slice_fusion.2
  259.0 0.6 convolution_bitcast_fusion.3
  259.7 1.3 fusion.109
  261.0 0.6 convolution_add_fusion.3
  261.7 1.5 copy.86
  263.2 0.2 reshape.58
  263.9 21.1 %all-gather.20.cloned.1.call-done = bf16[512,2048]{1,0:T(8,128)(2,1)} async-done(((bf16[512,256]{1,0:T(8,128)(2,1)}), bf16[512,2048]{1,0:T(8,128)(2,1)}) %all-gather.20.cloned.1.call-update) | async-done | bytes 2097168 | tf_op jit(solution)/shard_map/all_gather | solution.py:151
  285.0 4.4 convolution_convert_fusion.3
  289.5 0.7 all-gather.24.cloned.1.call-update
  290.3 0.7 all-gather.22.cloned.1.call-update
  291.0 0.5 all-gather.26.cloned.1.call-update
  291.7 4.3 reduce-scatter.3.cloned.1.call-done
  296.0 1.1 add_convert_fusion.1
  297.1 2.5 all_gather.40
  299.6 0.2 fusion.32
  299.9 123.8 %all-gather.24.cloned.1.call-done = bf16[2048,2048]{1,0:T(8,128)(2,1)} async-done(((bf16[256,2048]{1,0:T(8,128)(2,1)}), bf16[2048,2048]{1,0:T(8,128)(2,1)}) %all-gather.24.cloned.1.call-update) | async-done | bytes 8388624 | tf_op jit(solution)/shard_map/all_gather | solution.py:164
  423.7 5.2 fusion.17
  428.9 119.6 %all-gather.22.cloned.1.call-done = bf16[2048,2048]{1,0:T(8,128)(2,1)} async-done(((bf16[256,2048]{1,0:T(8,128)(2,1)}), bf16[2048,2048]{1,0:T(8,128)(2,1)}) %all-gather.22.cloned.1.call-update) | async-done | bytes 8388624 | tf_op jit(solution)/shard_map/all_gather | solution.py:163
  548.5 6.4 fusion.18
  554.9 118.6 %all-gather.26.cloned.1.call-done = bf16[2048,2048]{1,0:T(8,128)(2,1)} async-done(((bf16[2048,256]{1,0:T(8,128)(2,1)}), bf16[2048,2048]{1,0:T(8,128)(2,1)}) %all-gather.26.cloned.1.call-update) | async-done | bytes 8388624 | tf_op jit(solution)/shard_map/all_gather | solution.py:174
  673.6 9.0 %convolution_convert_fusion = bf16[192,2048]{1,0:T(8,128)(2,1)} fusion(bf16[2048,2048]{1,0:T(8,128)(2,1)} %all-gather.26.cloned.1.call-done, f32[192,2048]{1,0:T(8,128)} %fusion.18, f32[192,2048]{1,0:T(8,128)S(1)} %fusion.17, f32[2048]{0:T(1024)S(1)} %bitcast.92, f32[2048]{0:T(1024)S(1)} %bitcast.91, f32[2048]{0:T(1024)S(1)} %bitcast.90, ...), kind=kOutput, calls=%fused_computation.29 | convolution fusion | flops 1618870272 | bytes 12369920 | tf_op jit(solution)/shard_map/dot_general | solution.py:172
  682.7 6.5 reduce-scatter.5.cloned.1.call-done
  689.1 1.9 add_convert_fusion
  (75 shorter events, 2.6 us)
Async XLA Ops:
  6.5 7.0 %copy-start.6 = (bf16[2048]{0:T(1024)(128)(2,1)S(1)}, bf16[2048]{0:T(1024)(128)(2,1)}, u32[]{:S(2)}) copy-start(bf16[2048]{0:T(1024)(128)(2,1)} %param.20) | copy-start | bytes 12292
  6.5 7.0 %copy-start.8 = (bf16[512]{0:T(512)(128)(2,1)S(1)}, bf16[512]{0:T(512)(128)(2,1)}, u32[]{:S(2)}) copy-start(bf16[512]{0:T(512)(128)(2,1)} %param.28) | copy-start | bytes 3076
  6.5 46.0 %copy-start.9 = (f32[192,256]{1,0:T(8,128)S(1)}, f32[192,256]{1,0:T(8,128)}, u32[]{:S(2)}) copy-start(f32[192,256]{1,0:T(8,128)} %param.27) | copy-start | bytes 589828
  6.5 46.0 %copy-start.10 = (f32[256]{0:T(256)S(1)}, f32[256]{0:T(256)}, u32[]{:S(2)}) copy-start(f32[256]{0:T(256)} %param.26) | copy-start | bytes 3076
  6.5 46.0 %all-gather.10.cloned.1.call-start = ((), (), s32[]{:S(2)}) async-start(), calls=%async_computation.2 | async-start | bytes 1179648 | tf_op jit(solution)/shard_map/all_gather | solution.py:133
  7.3 86.4 %all-gather.12.cloned.1.call-start = ((), (), s32[]{:S(2)}) async-start(), calls=%async_computation.3 | async-start | bytes 1179648 | tf_op jit(solution)/shard_map/all_gather | solution.py:131
  8.0 126.8 %all-gather.16.cloned.1.call-start = ((), (), s32[]{:S(2)}) async-start(), calls=%async_computation.5 | async-start | bytes 1179648 | tf_op jit(solution)/shard_map/all_gather | solution.py:130
  8.8 175.9 %all-gather.14.cloned.1.call-start = ((), (), s32[]{:S(2)}) async-start(), calls=%async_computation.4 | async-start | bytes 2359296 | tf_op jit(solution)/shard_map/all_gather | solution.py:132
  9.3 254.6 %all-gather.18.cloned.1.call-start = ((), (), s32[]{:S(2)}) async-start(), calls=%async_computation.6 | async-start | bytes 2359296 | tf_op jit(solution)/shard_map/all_gather | solution.py:134
  9.9 275.1 %all-gather.20.cloned.1.call-start = ((), (), s32[]{:S(2)}) async-start(), calls=%async_computation.7 | async-start | bytes 2359296 | tf_op jit(solution)/shard_map/all_gather | solution.py:151
  10.5 285.5 %reduce-scatter.3.cloned.1.call-start = ((), (), s32[]{:S(2)}) async-start(), calls=%async_computation.8 | async-start | bytes 1179648 | tf_op jit(solution)/shard_map/reduce_scatter | solution.py:154
  13.3 171.4 %copy-start = (bf16[192,2048]{1,0:T(8,128)(2,1)}, bf16[192,2048]{1,0:T(8,128)(2,1)S(1)}, u32[]{:S(2)}) copy-start(bf16[192,2048]{1,0:T(8,128)(2,1)S(1)} %all_gather.33) | copy-start | bytes 2359300
  261.7 1.8 copy-start.2
  263.2 21.8 %copy-start.1 = (bf16[192,2048]{1,0:T(8,128)(2,1)S(1)}, bf16[192,2048]{1,0:T(8,128)(2,1)}, u32[]{:S(2)}) copy-start(bf16[192,2048]{1,0:T(8,128)(2,1)} %copy-done) | copy-start | bytes 2359300
  289.4 2.2 copy-start.7
  289.4 2.2 copy-start.4
  289.5 2.2 copy-start.5
  289.5 6.5 copy-start.3
  289.5 134.2 %all-gather.24.cloned.1.call-start = ((), (), s32[]{:S(2)}) async-start(), calls=%async_computation.10 | async-start | bytes 9437184 | tf_op jit(solution)/shard_map/all_gather | solution.py:164
  290.2 258.3 %all-gather.22.cloned.1.call-start = ((), (), s32[]{:S(2)}) async-start(), calls=%async_computation.9 | async-start | bytes 9437184 | tf_op jit(solution)/shard_map/all_gather | solution.py:163
  291.0 382.6 %all-gather.26.cloned.1.call-start = ((), (), s32[]{:S(2)}) async-start(), calls=%async_computation.11 | async-start | bytes 9437184 | tf_op jit(solution)/shard_map/all_gather | solution.py:174
  291.5 397.6 %reduce-scatter.5.cloned.1.call-start = ((), (), s32[]{:S(2)}) async-start(), calls=%async_computation.12 | async-start | bytes 1179648 | tf_op jit(solution)/shard_map/reduce_scatter | solution.py:177
Sparse Core Ops, SparseCore 0:
  9.5 42.9 all-gather.9
  54.6 38.9 all-gather.11
  95.8 38.9 all-gather.15
  136.8 47.7 all-gather.13
  186.6 47.6 all-gather.17
  236.1 48.8 all-gather.19
  289.5 6.3 reduce-scatter.2
  298.1 125.5 all-gather.23
  425.8 122.6 all-gather.21
  550.4 123.1 all-gather.25
  682.8 6.3 reduce-scatter.4
where the time goes:
time: 699 us; the launch traced here: 698 us
  waiting for transfers between devices  564 us (81%)
  matrix products  39.9 us (6%)
  local copies, waits for them, and re-layouts  37.6 us (5%)
  other arithmetic  36.7 us (5%)
  between operations  13.5 us (2%)
    all_gather x1, waiting for transfers between devices, shards(): lax.all_gather(switch_expand_matrix, 'fs', axis=0, tiled=True)  124 us
    all_gather x1, waiting for transfers between devices, shards(): lax.all_gather(content_expand_matrix, 'fs', axis=0, tiled=True)  120 us
    all_gather x1, waiting for transfers between devices, shards(): lax.all_gather(contract_matrix, 'fs', axis=1, tiled=True)  119 us
    all_gather x1, waiting for transfers between devices, shards(): lax.all_gather(content_matrix, 'fs', axis=0, tiled=True)  47.9 us
    all_gather x1, waiting for transfers between devices, shards(): lax.all_gather(probe_matrix, 'fs', axis=0, tiled=True)  39.3 us
    all_gather x1, waiting for transfers between devices, shards(): lax.all_gather(forgetting_matrix, 'fs', axis=0, tiled=True)  39 us
    all_gather x1, waiting for transfers between devices, shards(): lax.all_gather(lookup_matrix, 'fs', axis=0, tiled=True)  38.2 us
    while x3, local copies, waits for them, and re-layouts  28.6 us
  transfers between devices with their start and end apart: 11, of which 10 were waited for; matrix products, arithmetic and copies ran while one was open for 14% of the time, Pallas kernels for 0%

commit v1 on v0

--- a/solution.py
+++ b/solution.py
@@ -171,7 +171,7 @@
     hidden = (conv_value * jax.nn.gelu(conv_gated, approximate=True)).astype(jnp.bfloat16)
     down_partial = jnp.dot(
         hidden,
-        lax.all_gather(contract_matrix, "fs", axis=1, tiled=True),
+        jnp.concatenate(lax.all_gather(contract_matrix, "fs"), axis=1),
         preferred_element_type=jnp.float32,
     )
     ffn = lax.psum_scatter(down_partial.astype(jnp.bfloat16), "tp", scatter_dimension=1, tiled=True)

time: 699 us -> 700 us (level)
  local copies, waits for them, and re-layouts: 37.6 us -> 49.7 us
    reshape x0 -> x1, local copies, waits for them, and re-layouts: none -> 11.7 us  [shards(): jnp.concatenate(lax.all_gather(contract_matrix, 'fs'), axis=1)]
    all_gather x1, waiting for transfers between devices: 124 us -> 113 us  [shards(): lax.all_gather(switch_expand_matrix, 'fs', axis=0, tiled=True)]
  transfers between devices with their start and end apart: 11 -> 11, of which waited for: 10 -> 10; matrix products, arithmetic and copies ran while one was open for 14% -> 15% of each run, Pallas kernels for 0% -> 0%
where the time goes in v1:
time: 700 us; the launch traced here: 699 us
  waiting for transfers between devices  558 us (80%)
  local copies, waits for them, and re-layouts  49.7 us (7%)
  other arithmetic  36.6 us (5%)
  matrix products  34.5 us (5%)
  between operations  13.5 us (2%)
    all_gather x1, waiting for transfers between devices, shards(): lax.all_gather(contract_matrix, 'fs')  124 us
    all_gather x1, waiting for transfers between devices, shards(): lax.all_gather(content_expand_matrix, 'fs', axis=0, tiled=True)  119 us
    all_gather x1, waiting for transfers between devices, shards(): lax.all_gather(switch_expand_matrix, 'fs', axis=0, tiled=True)  113 us
    all_gather x1, waiting for transfers between devices, shards(): lax.all_gather(content_matrix, 'fs', axis=0, tiled=True)  47.9 us
    all_gather x1, waiting for transfers between devices, shards(): lax.all_gather(probe_matrix, 'fs', axis=0, tiled=True)  39.3 us
    all_gather x1, waiting for transfers between devices, shards(): lax.all_gather(forgetting_matrix, 'fs', axis=0, tiled=True)  39 us
    all_gather x1, waiting for transfers between devices, shards(): lax.all_gather(lookup_matrix, 'fs', axis=0, tiled=True)  38.2 us
    while x3, local copies, waits for them, and re-layouts  28.6 us
  transfers between devices with their start and end apart: 11, of which 10 were waited for; matrix products, arithmetic and copies ran while one was open for 15% of the time, Pallas kernels for 0%

profile of v1, /device:TPU:0, one launch (start us, length us, event | category | flops | bytes accessed | tf_op | source)
XLA Modules:
  0.0 698.6 jit_solution(8128798606076120107)
XLA Ops:
  6.6 0.7 all-gather.11.cloned.1.call-update
  7.3 0.7 all-gather.13.cloned.1.call-update
  8.1 0.7 all-gather.17.cloned.1.call-update
  8.8 0.5 all-gather.15.cloned.1.call-update
  9.4 0.5 all-gather.19.cloned.1.call-update
  10.0 0.5 all-gather.21.cloned.1.call-update
  10.6 2.7 all_gather.36
  13.3 0.2 fusion.29
  13.5 39.0 %all-gather.11.cloned.1.call-done = bf16[2048,256]{1,0:T(8,128)(2,1)} async-done(((bf16[256,256]{1,0:T(8,128)(2,1)}), bf16[2048,256]{1,0:T(8,128)(2,1)}) %all-gather.11.cloned.1.call-update) | async-done | bytes 1048592 | tf_op jit(solution)/shard_map/all_gather | solution.py:133
  52.5 1.7 fusion.65
  54.3 1.1 reshape.73
  55.4 38.2 %all-gather.13.cloned.1.call-done = bf16[2048,256]{1,0:T(8,128)(2,1)} async-done(((bf16[256,256]{1,0:T(8,128)(2,1)}), bf16[2048,256]{1,0:T(8,128)(2,1)}) %all-gather.13.cloned.1.call-update) | async-done | bytes 1048592 | tf_op jit(solution)/shard_map/all_gather | solution.py:131
  93.7 1.7 fusion.47
  95.3 0.2 reshape.74
  95.5 39.3 %all-gather.17.cloned.1.call-done = bf16[2048,256]{1,0:T(8,128)(2,1)} async-done(((bf16[256,256]{1,0:T(8,128)(2,1)}), bf16[2048,256]{1,0:T(8,128)(2,1)}) %all-gather.17.cloned.1.call-update) | async-done | bytes 1048592 | tf_op jit(solution)/shard_map/all_gather | solution.py:130
  134.8 1.7 fusion.46
  136.7 47.9 %all-gather.15.cloned.1.call-done = bf16[2048,512]{1,0:T(8,128)(2,1)} async-done(((bf16[256,512]{1,0:T(8,128)(2,1)}), bf16[2048,512]{1,0:T(8,128)(2,1)}) %all-gather.15.cloned.1.call-update) | async-done | bytes 2097168 | tf_op jit(solution)/shard_map/all_gather | solution.py:132
  184.6 2.2 fusion.43
  186.8 1.1 reshape.68
  187.9 73.6 %while.13 = (s32[]{:T(128)}, f32[8,32,64]{2,1,0:T(8,128)S(1)}, f32[3,64,8,64]{1,3,2,0:T(8,128)}, f32[3,64,8,32]{3,2,1,0:T(8,128)}, f32[3,64,8,32]{3,2,1,0:T(8,12...) while((s32[]{:T(128)}, f32[8,32,64]{2,1,0:T(8,128)S(1)}, ...), condition=%wide.region_3.4_spmd.clone, body=%wide.region_1.3_spmd.clone.sunk | while | flops 56725504 | bytes 20003956 | solution.py:52
  187.9 1.0 fusion.106
  189.1 4.6 select_exponential_fusion.2
  193.7 9.5 %copy.125 = f32[64,64,8,32]{0,1,3,2:T(8,128)} copy(f32[64,64,8,32]{1,3,2,0:T(8,128)} %select_exponential_fusion.2) | data formatting | bytes 8388608 | tf_op jit(solution)/shard_map/while
  203.5 5.3 fusion.108
  208.8 1.0 constant_dynamic-slice_fusion.2
  209.7 0.6 convolution_bitcast_fusion.3
  210.4 1.3 fusion.109
  211.8 0.6 convolution_add_fusion.3
  212.4 1.0 fusion.106
  213.6 4.6 select_exponential_fusion.2
  218.2 9.5 %copy.125 = f32[64,64,8,32]{0,1,3,2:T(8,128)} copy(f32[64,64,8,32]{1,3,2,0:T(8,128)} %select_exponential_fusion.2) | data formatting | bytes 8388608 | tf_op jit(solution)/shard_map/while
  228.0 5.2 fusion.108
  233.3 1.0 constant_dynamic-slice_fusion.2
  234.3 0.6 convolution_bitcast_fusion.3
  235.0 1.3 fusion.109
  236.3 0.6 convolution_add_fusion.3
  236.9 1.0 fusion.106
  238.1 4.6 select_exponential_fusion.2
  242.7 9.6 %copy.125 = f32[64,64,8,32]{0,1,3,2:T(8,128)} copy(f32[64,64,8,32]{1,3,2,0:T(8,128)} %select_exponential_fusion.2) | data formatting | bytes 8388608 | tf_op jit(solution)/shard_map/while
  252.6 5.3 fusion.108
  257.9 1.0 constant_dynamic-slice_fusion.2
  258.8 0.6 convolution_bitcast_fusion.3
  259.5 1.3 fusion.109
  260.9 0.6 convolution_add_fusion.3
  261.5 1.5 copy.88
  263.7 21.3 %all-gather.21.cloned.1.call-done = bf16[512,2048]{1,0:T(8,128)(2,1)} async-done(((bf16[512,256]{1,0:T(8,128)(2,1)}), bf16[512,2048]{1,0:T(8,128)(2,1)}) %all-gather.21.cloned.1.call-update) | async-done | bytes 2097168 | tf_op jit(solution)/shard_map/all_gather | solution.py:151
  285.1 4.4 convolution_convert_fusion.3
  289.6 0.7 all-gather.27.cloned.1.call-update
  290.3 0.7 all-gather.25.cloned.1.call-update
  291.1 0.5 all-gather.23.cloned.1.call-update
  291.7 4.2 reduce-scatter.3.cloned.1.call-done
  295.9 1.1 add_convert_fusion.1
  297.1 2.5 all_gather.43
  299.6 0.2 fusion.32
  299.9 123.8 %all-gather.27.cloned.1.call-done = bf16[16384,256]{1,0:T(8,128)(2,1)} async-done(((bf16[2048,256]{1,0:T(8,128)(2,1)}), bf16[16384,256]{1,0:T(8,128)(2,1)}) %all-gather.27.cloned.1.call-update) | async-done | bytes 8388624 | tf_op jit(solution)/shard_map/all_gather | solution.py:174
  423.7 11.7 %copy.91 = bf16[2048,8,256]{0,2,1:T(8,128)(2,1)} copy(bf16[2048,8,256]{2,0,1:T(8,128)(2,1)} %bitcast.90) | data formatting | bytes 16777216 | tf_op jit(solution)/shard_map/reshape | solution.py:174
  435.4 113.1 %all-gather.25.cloned.1.call-done = bf16[2048,2048]{1,0:T(8,128)(2,1)} async-done(((bf16[256,2048]{1,0:T(8,128)(2,1)}), bf16[2048,2048]{1,0:T(8,128)(2,1)}) %all-gather.25.cloned.1.call-update) | async-done | bytes 8388624 | tf_op jit(solution)/shard_map/all_gather | solution.py:164
  548.5 5.2 fusion.17
  553.8 119.4 %all-gather.23.cloned.1.call-done = bf16[2048,2048]{1,0:T(8,128)(2,1)} async-done(((bf16[256,2048]{1,0:T(8,128)(2,1)}), bf16[2048,2048]{1,0:T(8,128)(2,1)}) %all-gather.23.cloned.1.call-update) | async-done | bytes 8388624 | tf_op jit(solution)/shard_map/all_gather | solution.py:163
  673.2 5.4 fusion.18
  678.6 0.4 copy-done
  679.0 4.7 convolution_convert_fusion
  683.7 6.5 reduce-scatter.5.cloned.1.call-done
  690.2 1.9 add_convert_fusion
  (78 shorter events, 3.1 us)
Async XLA Ops:
  6.5 7.0 copy-start.7
  6.5 7.0 %copy-start.9 = (bf16[512]{0:T(512)(128)(2,1)S(1)}, bf16[512]{0:T(512)(128)(2,1)}, u32[]{:S(2)}) copy-start(bf16[512]{0:T(512)(128)(2,1)} %param.28) | copy-start | bytes 3076
  6.5 46.0 %copy-start.10 = (f32[192,256]{1,0:T(8,128)S(1)}, f32[192,256]{1,0:T(8,128)}, u32[]{:S(2)}) copy-start(f32[192,256]{1,0:T(8,128)} %param.27) | copy-start | bytes 589828
  6.5 46.0 %copy-start.11 = (f32[256]{0:T(256)S(1)}, f32[256]{0:T(256)}, u32[]{:S(2)}) copy-start(f32[256]{0:T(256)} %param.26) | copy-start | bytes 3076
  6.5 46.0 %all-gather.11.cloned.1.call-start = ((), (), s32[]{:S(2)}) async-start(), calls=%async_computation.2 | async-start | bytes 1179648 | tf_op jit(solution)/shard_map/all_gather | solution.py:133
  7.3 86.4 %all-gather.13.cloned.1.call-start = ((), (), s32[]{:S(2)}) async-start(), calls=%async_computation.3 | async-start | bytes 1179648 | tf_op jit(solution)/shard_map/all_gather | solution.py:131
  8.0 126.8 %all-gather.17.cloned.1.call-start = ((), (), s32[]{:S(2)}) async-start(), calls=%async_computation.5 | async-start | bytes 1179648 | tf_op jit(solution)/shard_map/all_gather | solution.py:130
  8.8 175.9 %all-gather.15.cloned.1.call-start = ((), (), s32[]{:S(2)}) async-start(), calls=%async_computation.4 | async-start | bytes 2359296 | tf_op jit(solution)/shard_map/all_gather | solution.py:132
  9.3 254.4 %all-gather.19.cloned.1.call-start = ((), (), s32[]{:S(2)}) async-start(), calls=%async_computation.6 | async-start | bytes 2359296 | tf_op jit(solution)/shard_map/all_gather | solution.py:134
  9.9 275.1 %all-gather.21.cloned.1.call-start = ((), (), s32[]{:S(2)}) async-start(), calls=%async_computation.7 | async-start | bytes 2359296 | tf_op jit(solution)/shard_map/all_gather | solution.py:151
  10.5 285.4 %reduce-scatter.3.cloned.1.call-start = ((), (), s32[]{:S(2)}) async-start(), calls=%async_computation.8 | async-start | bytes 1179648 | tf_op jit(solution)/shard_map/reduce_scatter | solution.py:154
  13.3 171.4 %copy-start.1 = (bf16[192,2048]{1,0:T(8,128)(2,1)}, bf16[192,2048]{1,0:T(8,128)(2,1)S(1)}, u32[]{:S(2)}) copy-start(bf16[192,2048]{1,0:T(8,128)(2,1)S(1)} %all_gather.36) | copy-start | bytes 2359300
  261.5 1.8 copy-start.3
  263.0 22.0 %copy-start.2 = (bf16[192,2048]{1,0:T(8,128)(2,1)S(1)}, bf16[192,2048]{1,0:T(8,128)(2,1)}, u32[]{:S(2)}) copy-start(bf16[192,2048]{1,0:T(8,128)(2,1)} %copy-done.1) | copy-start | bytes 2359300
  289.5 2.2 copy-start.8
  289.5 2.2 copy-start.5
  289.5 2.2 copy-start.6
  289.5 6.4 copy-start.4
  289.5 134.2 %all-gather.27.cloned.1.call-start = ((), (), s32[]{:S(2)}) async-start(), calls=%async_computation.12 | async-start | bytes 9437184 | tf_op jit(solution)/shard_map/all_gather | solution.py:174
  290.3 258.3 %all-gather.25.cloned.1.call-start = ((), (), s32[]{:S(2)}) async-start(), calls=%async_computation.10 | async-start | bytes 9437184 | tf_op jit(solution)/shard_map/all_gather | solution.py:164
  291.0 382.2 %all-gather.23.cloned.1.call-start = ((), (), s32[]{:S(2)}) async-start(), calls=%async_computation.9 | async-start | bytes 9437184 | tf_op jit(solution)/shard_map/all_gather | solution.py:163
  291.6 398.6 %reduce-scatter.5.cloned.1.call-start = ((), (), s32[]{:S(2)}) async-start(), calls=%async_computation.11 | async-start | bytes 1179648 | tf_op jit(solution)/shard_map/reduce_scatter | solution.py:177
  673.2 5.8 copy-start
Sparse Core Ops, SparseCore 0:
  9.5 42.9 all-gather.10
  54.6 38.9 all-gather.12
  95.8 38.9 all-gather.16
  136.8 47.7 all-gather.14
  186.6 47.6 all-gather.18
  236.1 48.8 all-gather.20
  289.6 6.2 reduce-scatter.2
  298.1 125.6 all-gather.26
  425.8 122.6 all-gather.24
  550.5 122.6 all-gather.22
  683.8 6.3 reduce-scatter.4
